TPU v7x, 32 devices: a whole 2x2x4 slice. The times are simulated.
32 devices in a mesh: sp: 8 (over z, x), tp: 4 (over y, core).
Axes of the slice: x: 2, y: 2, z: 4, core: 2. Of those that a mesh axis runs over, the one named last changes fastest.
Arguments:
- target_rows: bfloat16 [512, 2048], P(('sp', 'tp')), may hold values from -6 to 6
- source_rows: bfloat16 [2048, 2048], P(('sp', 'tp')), may hold values from -6 to 6
- norm_gain: bfloat16 [2048], replicated, may hold values from 0.099609375 to 1.8984375
- query_weight: bfloat16 [2048, 4096], P(None, 'tp'), may hold values from -0.125 to 0.125
- key_weight: bfloat16 [2048, 4096], P(None, 'tp'), may hold values from -0.125 to 0.125
- value_weight: bfloat16 [2048, 4096], P(None, 'tp'), may hold values from -0.125 to 0.125
- output_weight: bfloat16 [4096, 2048], P('tp'), may hold values from -0.09375 to 0.09375
- saved_output: bfloat16 [512, 4096], P('sp', 'tp'), may hold values from -3 to 3
- norm_offset: bfloat16 [512, 16], P('sp', 'tp'), may hold values from 0.25 to 1.25
- output_grad: bfloat16 [512, 2048], P(('sp', 'tp')), may hold values from -192 to 192
Outputs:
- target_grad: float32 [512, 2048], P(('sp', 'tp'))
- source_grad: float32 [2048, 2048], P(('sp', 'tp'))
- query_weight_grad: float32 [2048, 4096], P('sp', 'tp')
All inputs are finite; a program needn't handle non-finite values.
Results may differ from a plain program's by a relative error of at most 0.033.
Values may be sent and summed in bfloat16 or wider, within the bound.
A program may use at most 64 MiB of HBM per device.

v0:
```python
import math

import jax
import jax.numpy as jnp
from jax import lax
from jax.sharding import PartitionSpec as P

HEAD_DIM = 256


EPSILON = 1e-06


def contract_last(left, right):
    return lax.dot_general(
        left, right, (((1,), (1,)), ((), ())), preferred_element_type=jnp.float32
    )


def attention_weights(
    query_rows, head_gradient, offsets, deltas, key_row_block, value_row_block, shift_base
):
    score_scale = HEAD_DIM ** (-0.5)
    score_matrix = jnp.einsum(
        "rfo,kfo->frk", query_rows, key_row_block, preferred_element_type=jnp.float32
    )
    shifts = jnp.transpose(shift_base + offsets.astype(jnp.float32))[:, :, None]
    prob_rows = jnp.exp(score_matrix * score_scale - shifts)
    prob_grad = jnp.einsum(
        "rfo,kfo->frk", head_gradient, value_row_block, preferred_element_type=jnp.float32
    )
    score_grad = (
        prob_rows
        * (prob_grad - jnp.transpose(deltas.astype(jnp.float32))[:, :, None])
        * score_scale
    )
    return (prob_rows.astype(jnp.bfloat16), score_grad.astype(jnp.bfloat16))


def body(
    target_rows,
    source_rows,
    norm_gain,
    query_weight,
    key_weight,
    value_weight,
    output_weight,
    saved_output,
    norm_offset,
    output_grad,
):
    tp_count = lax.axis_size("tp")
    sp_count = lax.axis_size("sp")
    query_width = query_weight.shape[1]
    local_heads = query_width // HEAD_DIM
    target_count = saved_output.shape[0]
    source_count = source_rows.shape[0] * tp_count
    shift_base = math.log(source_count * sp_count)
    target_float = target_rows.astype(jnp.float32)
    gain_float = norm_gain.astype(jnp.float32)
    inverse = lax.rsqrt(jnp.mean(target_float * target_float, axis=1, keepdims=True) + EPSILON)
    normed = (target_float * inverse * gain_float).astype(jnp.bfloat16)
    slice_share = lax.all_gather(jnp.stack([normed, output_grad]), "tp", axis=1, tiled=True)
    query_part = jnp.dot(slice_share[0], query_weight, preferred_element_type=jnp.float32).astype(
        jnp.bfloat16
    )
    grad_part = contract_last(slice_share[1], output_weight).astype(jnp.bfloat16)
    joined = jnp.concatenate([query_part, grad_part, slice_share[0]], axis=1)
    query_rows = joined[:, :query_width].reshape(target_count, local_heads, HEAD_DIM)
    head_gradient = joined[:, query_width : 2 * query_width].reshape(
        target_count, local_heads, HEAD_DIM
    )
    normed_all = joined[:, 2 * query_width :]
    saved_heads = saved_output.reshape(target_count, local_heads, HEAD_DIM)
    deltas = jnp.sum(
        head_gradient.astype(jnp.float32) * saved_heads.astype(jnp.float32), axis=2
    ).astype(jnp.bfloat16)
    slice_share = lax.all_gather(source_rows, "tp", axis=0, tiled=True)
    key_part = jnp.dot(slice_share, key_weight, preferred_element_type=jnp.float32).astype(
        jnp.bfloat16
    )
    value_part = jnp.dot(slice_share, value_weight, preferred_element_type=jnp.float32).astype(
        jnp.bfloat16
    )
    projected = jnp.concatenate([key_part, value_part], axis=1)
    key_row_block = projected[:, :query_width].reshape(source_count, local_heads, HEAD_DIM)
    value_row_block = projected[:, query_width:].reshape(source_count, local_heads, HEAD_DIM)
    slice_share = (
        lax.all_gather(query_rows, "sp", axis=0, tiled=True),
        lax.all_gather(head_gradient, "sp", axis=0, tiled=True),
        lax.all_gather(norm_offset, "sp", axis=0, tiled=True),
        lax.all_gather(deltas, "sp", axis=0, tiled=True),
    )
    probability_rounded, score_rounded = attention_weights(
        slice_share[0],
        slice_share[1],
        slice_share[2],
        slice_share[3],
        key_row_block,
        value_row_block,
        shift_base,
    )
    key_total = jnp.einsum(
        "wcu,cwp->uwp", score_rounded, slice_share[0], preferred_element_type=jnp.float32
    )
    value_total = jnp.einsum(
        "wcu,cwp->uwp", probability_rounded, slice_share[1], preferred_element_type=jnp.float32
    )
    key_total, value_total, score_rounded = (key_total, value_total, score_rounded)
    query_term = jnp.einsum(
        "tje,etq->jtq", score_rounded, key_row_block, preferred_element_type=jnp.float32
    )
    query_grad = lax.psum_scatter(query_term, "sp", scatter_dimension=0, tiled=True)
    query_flat = query_grad.astype(jnp.bfloat16).reshape(target_count, query_width)
    normed_grad = lax.psum_scatter(
        contract_last(query_flat, query_weight), "tp", scatter_dimension=0, tiled=True
    )
    scaled = normed_grad * gain_float
    target_grad = inverse * scaled - target_float * inverse**3 * jnp.mean(
        scaled * target_float, axis=1, keepdims=True
    )
    key_flat = key_total.astype(jnp.bfloat16).reshape(source_count, query_width)
    value_flat = value_total.astype(jnp.bfloat16).reshape(source_count, query_width)
    key_part = contract_last(key_flat, key_weight)
    value_part = contract_last(value_flat, value_weight)
    source_grad = lax.psum_scatter(key_part + value_part, "tp", scatter_dimension=0, tiled=True)
    weight_grad = lax.psum_scatter(
        lax.dot_general(
            normed_all, query_flat, (((0,), (0,)), ((), ())), preferred_element_type=jnp.float32
        ),
        "sp",
        scatter_dimension=0,
        tiled=True,
    )
    return (target_grad, source_grad, weight_grad)


def solution(mesh):
    in_specs = (
        P(("sp", "tp"), None),
        P(("sp", "tp"), None),
        P(),
        P(None, "tp"),
        P(None, "tp"),
        P(None, "tp"),
        P("tp", None),
        P("sp", "tp"),
        P("sp", "tp"),
        P(("sp", "tp"), None),
    )
    out_specs = (P(("sp", "tp"), None), P(("sp", "tp"), None), P("sp", "tp"))
    return jax.shard_map(body, mesh=mesh, in_specs=in_specs, out_specs=out_specs, check_vma=False)
```

profile of v0, /device:TPU:0, one launch (start us, length us, event | category | flops | bytes accessed | tf_op | source)
XLA Modules:
  0.0 430.3 jit_solution(16171645265779175669)
XLA Ops:
  7.2 0.7 all-gather.6.cloned.1.call-update
  7.9 0.7 convert_element_type.60
  8.6 1.0 fusion.7
  9.6 0.9 fusion.13
  10.5 0.9 pad_maximum_fusion
  11.4 8.7 %all_gather.19 = bf16[2,64,2048]{2,1,0:T(8,128)(2,1)S(1)} all-gather(bf16[2,16,2048]{2,1,0:T(8,128)(2,1)S(1)} %pad_maximum_fusion), channel_id=1, replica_groups=mesh['sp'=8,'tp'=4] {'tp'}, dimensions={1}, use_global_device_ids=true | all-gather | bytes 655360 | tf_op jit(solution)/shard_map/all_gather | solution.py:63
  20.1 3.2 convolution_convert_fusion.5
  24.1 3.6 convolution_convert_fusion.4
  27.7 0.7 copy.63
  28.5 20.8 %all-gather = bf16[8,64,4]{1,2,0:T(4,128)(2,1)S(1)} all-gather(bf16[1,64,4]{1,2,0:T(4,128)(2,1)S(1)} %bitcast.79), channel_id=1, replica_groups=mesh['sp'=8,'tp'=4] {'sp'}, dimensions={0}, use_global_device_ids=true | all-gather | bytes 4608 | tf_op jit(solution)/shard_map/all_gather | solution.py:91
  49.8 16.3 %all-gather.1 = bf16[8,64,4]{1,2,0:T(4,128)(2,1)S(1)} all-gather(bf16[1,64,4]{1,2,0:T(4,128)(2,1)S(1)} %bitcast.78), channel_id=1, replica_groups=mesh['sp'=8,'tp'=4] {'sp'}, dimensions={0}, use_global_device_ids=true | all-gather | bytes 4608 | tf_op jit(solution)/shard_map/all_gather | solution.py:92
  67.5 3.8 convolution_convert_fusion.3
  71.6 3.4 convolution_convert_fusion.2
  75.0 1.7 fusion.15
  76.7 37.2 %all-gather.10.cloned.1.call-done = bf16[512,4,256]{2,0,1:T(8,128)(2,1)} async-done(((bf16[64,4,256]{2,0,1:T(8,128)(2,1)}), bf16[512,4,256]{2,0,1:T(8,128)(2,1)}) %all-gather.10.cloned.1.call-update) | async-done | bytes 1048592 | tf_op jit(solution)/shard_map/all_gather | solution.py:90
  113.9 1.9 multiply_convert_fusion
  115.9 1.0 copy-done.1
  116.8 1.8 convolution_bitcast_fusion
  118.6 2.9 copy.48
  121.5 91.2 %all-reduce.2 = bf16[512,4,256]{2,1,0:T(4,128)(2,1)S(1)} all-reduce(f32[512,4,256]{2,1,0:T(4,128)} %copy.48), channel_id=2, replica_groups=mesh['sp'=8,'tp'=4] {'sp'}, use_global_device_ids=true, to_apply=%region_2.0.clone | all-reduce | flops 524288 | bytes 3145728
  212.8 4.4 %fusion.16 = f32[64,2048]{1,0:T(8,128)} fusion(bf16[64,1024]{1,0:T(8,128)(2,1)S(1)} %bitcast.66, bf16[2048,1024]{1,0:T(8,128)(2,1)} %param.13), kind=kOutput, calls=%fused_computation.41 | convolution fusion | flops 268435456 | bytes 4849664 | tf_op jit(solution)/shard_map/dot_general | solution.py:15
  217.5 2.2 convolution_convert_fusion
  220.4 1.3 fusion.17
  221.8 0.9 copy-done.3
  222.7 2.7 convolution_add_fusion
  225.4 1.0 copy-done.5
  226.4 4.5 %fusion.6 = f32[2048,1024]{1,0:T(8,128)} fusion(bf16[64,1024]{1,0:T(8,128)(2,1)S(1)} %bitcast.67, bf16[2,64,2048]{2,1,0:T(8,128)(2,1)S(1)} %copy-done.5), kind=kOutput, calls=%fused_computation.19 | convolution fusion | flops 268435456 | bytes 8781824 | tf_op jit(solution)/shard_map/dot_general | solution.py:128
  230.9 6.9 %reduce-scatter.4.cloned.1.call-done = f32[16,2048]{1,0:T(8,128)} async-done(((f32[64,2048]{1,0:T(8,128)}), f32[16,2048]{1,0:T(8,128)}) %reduce-scatter.4.cloned.1.call-update) | async-done | bytes 131088 | tf_op jit(solution)/shard_map/reduce_scatter | solution.py:115
  237.8 1.0 fusion.12
  238.8 1.7 fusion.11
  240.5 31.5 %reduce-scatter.6.cloned.1.call-done = f32[64,2048]{1,0:T(8,128)} async-done(((f32[256,2048]{1,0:T(8,128)}), f32[64,2048]{1,0:T(8,128)}) %reduce-scatter.6.cloned.1.call-update) | async-done | bytes 524304 | tf_op jit(solution)/shard_map/reduce_scatter | solution.py:126
  272.0 151.5 %reduce-scatter.8.cloned.1.call-done = f32[256,1024]{1,0:T(8,128)} async-done(((f32[2048,1024]{1,0:T(8,128)}), f32[256,1024]{1,0:T(8,128)}) %reduce-scatter.8.cloned.1.call-update) | async-done | bytes 1048592 | tf_op jit(solution)/shard_map/reduce_scatter | solution.py:127
  (50 shorter events, 3.5 us)
Async XLA Ops:
  7.2 60.3 %all-gather.6.cloned.1.call-start = ((), (), s32[]{:S(2)}) async-start(), calls=%async_computation.3 | async-start | bytes 1310720 | tf_op jit(solution)/shard_map/all_gather | solution.py:78
  7.9 67.1 %all-gather.8.cloned.1.call-start = ((), (), s32[]{:S(2)}) async-start(), calls=%async_computation.4 | async-start | bytes 1179648 | tf_op jit(solution)/shard_map/all_gather | solution.py:89
  20.1 4.0 copy-start.4
  24.0 4.5 %copy-start.8 = (bf16[64,4]{0,1:T(4,128)(2,1)S(1)}, bf16[64,4]{0,1:T(4,128)(2,1)}, u32[]{:S(2)}) copy-start(bf16[64,4]{0,1:T(4,128)(2,1)} %param.18) | copy-start | bytes 1540
  24.0 25.4 %copy-start.7 = (bf16[64,1024]{1,0:T(8,128)(2,1)S(1)}, bf16[64,1024]{1,0:T(8,128)(2,1)}, u32[]{:S(2)}) copy-start(bf16[64,1024]{1,0:T(8,128)(2,1)} %param.17) | copy-start | bytes 393220
  24.0 42.2 %copy-start.11 = (u32[32]{0:T(128)S(1)}, u32[32]{0:T(128)}, u32[]{:S(2)}) copy-start(u32[32]{0:T(128)} %constant.16) | copy-start | bytes 388
  24.0 89.9 %all-gather.10.cloned.1.call-start = ((), (), s32[]{:S(2)}) async-start(), calls=%async_computation.5 | async-start | bytes 1179648 | tf_op jit(solution)/shard_map/all_gather | solution.py:90
  28.4 209.4 %reduce-scatter.4.cloned.1.call-start = ((), (), s32[]{:S(2)}) async-start(), calls=%async_computation.6 | async-start | bytes 655360 | tf_op jit(solution)/shard_map/reduce_scatter | solution.py:115
  67.5 4.1 copy-start.10
  115.9 1.0 copy-start.1
  217.2 2.5 copy-start
  217.2 54.7 %reduce-scatter.6.cloned.1.call-start = ((), (), s32[]{:S(2)}) async-start(), calls=%async_computation.7 | async-start | bytes 2621440 | tf_op jit(solution)/shard_map/reduce_scatter | solution.py:126
  217.5 2.2 copy-start.2
  217.5 2.9 copy-start.9
  220.4 2.3 copy-start.3
  225.4 1.0 copy-start.5
  225.4 198.1 %reduce-scatter.8.cloned.1.call-start = ((), (), s32[]{:S(2)}) async-start(), calls=%async_computation.8 | async-start | bytes 9437184 | tf_op jit(solution)/shard_map/reduce_scatter | solution.py:127
  230.9 6.9 %copy-start.6 = (bf16[16,2048]{1,0:T(8,128)(2,1)S(1)}, bf16[16,2048]{1,0:T(8,128)(2,1)}, u32[]{:S(2)}) copy-start(bf16[16,2048]{1,0:T(8,128)(2,1)} %param.10) | copy-start | bytes 196612
Sparse Core Ops, SparseCore 0:
  9.5 19.4 all-gather.5
  31.8 40.3 all-gather.7
  75.0 38.8 all-gather.9
  217.3 20.4 reduce-scatter.3
  240.8 31.1 reduce-scatter.5
  276.0 147.4 reduce-scatter.7
where the time goes:
time: 431 us; the launch traced here: 430 us
  waiting for transfers between devices  228 us (53%)
  blocking collectives  137 us (32%)
  matrix products  35.1 us (8%)
  between operations  15 us (3%)
  local copies, waits for them, and re-layouts  8.63 us (2%)
  other arithmetic  6.32 us (1%)
    reduce_scatter x1, waiting for transfers between devices, body(): lax.psum_scatter(lax.dot_general(normed_all, query_flat, (((0,), (0,)), (...  152 us
    unnamed x1, blocking collectives  91.2 us
    all_gather x1, waiting for transfers between devices, body(): lax.all_gather(head_gradient, 'sp', axis=0, tiled=True)  37.2 us
    reduce_scatter x1, waiting for transfers between devices, body(): lax.psum_scatter(key_part + value_part, 'tp', scatter_dimension=0, tiled=...  31.5 us
    all_gather x1, blocking collectives, body(): lax.all_gather(norm_offset, 'sp', axis=0, tiled=True)  20.8 us
    all_gather x1, blocking collectives, body(): lax.all_gather(deltas, 'sp', axis=0, tiled=True)  16.3 us
    dot_general x4, matrix products, contract_last(): lax.dot_general(left, right, (((1,), (1,)), ((), ())), preferred_element_...  12 us
    all_gather x1, blocking collectives, body(): lax.all_gather(jnp.stack([normed, output_grad]), 'tp', axis=1, tiled=True)  8.68 us
  transfers between devices with their start and end apart: 6, of which 4 were waited for; matrix products, arithmetic and copies ran while one was open for 8% of the time, Pallas kernels for 0%

commit v1 on v0

v1 whole, which is shorter than its diff:
```python
import functools
import math

import jax
import jax.numpy as jnp
from jax import lax
from jax.experimental import pallas as pl
from jax.experimental.pallas import tpu as pltpu
from jax.sharding import PartitionSpec as P

HEAD_DIM = 256
EPSILON = 1e-06
MESH = pl.DeviceIdType.MESH
BF = jnp.bfloat16
F32 = jnp.float32
VMEM = pl.BlockSpec(memory_space=pltpu.VMEM)


def contract_last(left, right):
    return lax.dot_general(left, right, (((1,), (1,)), ((), ())), preferred_element_type=F32)


def push(src, dst, send, recv, device):
    return pltpu.make_async_remote_copy(
        src_ref=src, dst_ref=dst, send_sem=send, recv_sem=recv, device_id=device, device_id_type=MESH
    )


def greet(devices):
    barrier = pltpu.get_barrier_semaphore()
    for device in devices:
        pl.semaphore_signal(barrier, inc=1, device_id=device, device_id_type=MESH)
    pl.semaphore_wait(barrier, len(devices))


class Place:
    def __init__(self, sp, tp):
        self.sp, self.tp, self.Z, self.Y = sp, tp, sp // 2, tp // 2
        self.s, self.t = lax.axis_index("sp"), lax.axis_index("tp")
        self.z, self.x = self.s // 2, self.s % 2
        self.y, self.c = self.t // 2, self.t % 2
        self.partner = (self.s, self.y * 2 + 1 - self.c)
        self.across = (self.z * 2 + 1 - self.x, self.t)

    def chip_y(self, d):
        return (self.s, lax.rem(self.y + d + self.Y, self.Y) * 2 + self.c)

    def chip_z(self, d):
        return (lax.rem(self.z + d + self.Z, self.Z) * 2 + self.x, self.t)


class LineGather:
    def __init__(self, place, pairs, up_s, up_r, dn_s, dn_r, x_s, x_r):
        self.p, self.pairs = place, pairs
        self.sems = (up_s, up_r, dn_s, dn_r, x_s, x_r)

    def up(self, n, d, own=False):
        p, (own_ref, all_ref) = self.p, self.pairs[n]
        block = p.s - 2 * (d - 1)
        src = own_ref if own else all_ref.at[block]
        return push(src, all_ref.at[block], self.sems[0].at[n, d], self.sems[1].at[n, d], (p.s + 2, p.t))

    def up_wait(self, n, d):
        p, (_, all_ref) = self.p, self.pairs[n]
        ref = all_ref.at[p.s - 2 * d]
        return push(ref, ref, self.sems[0].at[n, d], self.sems[1].at[n, d], (p.s - 2, p.t))

    def dn(self, n, d, own=False):
        p, (own_ref, all_ref) = self.p, self.pairs[n]
        block = p.s + 2 * (d - 1)
        src = own_ref if own else all_ref.at[block]
        return push(src, all_ref.at[block], self.sems[2].at[n, d], self.sems[3].at[n, d], (p.s - 2, p.t))

    def dn_wait(self, n, d):
        p, (_, all_ref) = self.p, self.pairs[n]
        ref = all_ref.at[p.s + 2 * d]
        return push(ref, ref, self.sems[2].at[n, d], self.sems[3].at[n, d], (p.s + 2, p.t))

    def over(self, n, d):
        p, (own_ref, all_ref) = self.p, self.pairs[n]
        block = p.s - 2 * d
        k = d + p.Z - 1
        src = own_ref if d == 0 else all_ref.at[block]
        return push(src, all_ref.at[block], self.sems[4].at[n, k], self.sems[5].at[n, k], p.across)

    def over_wait(self, n, d):
        p, (_, all_ref) = self.p, self.pairs[n]
        ref = all_ref.at[p.z * 2 + 1 - p.x - 2 * d]
        k = d + p.Z - 1
        return push(ref, ref, self.sems[4].at[n, k], self.sems[5].at[n, k], p.across)

    def start(self):
        p = self.p
        count = range(len(self.pairs))

        @pl.when(p.z + 1 < p.Z)
        def _():
            for n in count:
                self.up(n, 1, True).start()

        @pl.when(p.z >= 1)
        def _():
            for n in count:
                self.dn(n, 1, True).start()

        for n in count:
            self.over(n, 0).start()

    def step(self, d):
        p = self.p
        for n in range(len(self.pairs)):

            @pl.when(p.z - d >= 0)
            def _():
                self.up_wait(n, d).wait_recv()

                @pl.when(p.z + 1 < p.Z)
                def _():
                    self.up(n, d + 1).start()

                self.over(n, d).start()

            @pl.when(p.z + d < p.Z)
            def _():
                self.dn_wait(n, d).wait_recv()

                @pl.when(p.z >= 1)
                def _():
                    self.dn(n, d + 1).start()

                self.over(n, -d).start()

    def finish(self):
        p = self.p
        for n in range(len(self.pairs)):
            for d in range(p.Z):
                for sign in (1, -1) if d else (1,):

                    @pl.when((p.z - d >= 0) if sign > 0 else (p.z + d < p.Z))
                    def _():
                        self.over_wait(n, sign * d).wait_recv()
                        self.over(n, sign * d).wait_send()

            for d in range(1, p.Z):

                @pl.when(jnp.logical_and(p.z - d + 1 >= 0, p.z + 1 < p.Z))
                def _():
                    self.up(n, d).wait_send()

                @pl.when(jnp.logical_and(p.z + d - 1 < p.Z, p.z >= 1))
                def _():
                    self.dn(n, d).wait_send()


def line_sems(p_z, n):
    return [pltpu.SemaphoreType.DMA((n, p_z + 1))] * 4 + [pltpu.SemaphoreType.DMA((n, 2 * p_z))] * 2


def rows_kernel(sp, tp, tgt, src, pieces, tgt_all, src_all, cols, loc, ys, yr, ps, pr, es, er):
    p = Place(sp, tp)
    greet(
        [p.partner]
        + [p.chip_y(d) for d in range(1, p.Y)]
        + [(lax.rem(p.s + e, sp), p.t) for e in range(1, sp)]
    )

    def spot(t, j):
        if j == 0:
            return tgt_all.at[:, t]
        return src_all.at[t]

    own = (tgt, src)
    started = []
    for j in range(2):
        for d in range(1, p.Y):
            copy = push(own[j], spot(p.t, j), ys.at[j, d], yr.at[j, d], p.chip_y(d))
            copy.start()
            started.append(copy)
        copy = push(own[j], spot(p.t, j), ps.at[j, 0], pr.at[j, 0], p.partner)
        copy.start()
        started.append(copy)
    for e in range(1, sp):
        s = lax.rem(p.s + e, sp)
        copy = push(pieces.at[s], cols.at[p.s], es.at[e], er.at[e], (s, p.t))
        copy.start()
        started.append(copy)
    mine = [
        pltpu.make_async_copy(tgt, spot(p.t, 0), loc.at[0]),
        pltpu.make_async_copy(src, spot(p.t, 1), loc.at[1]),
        pltpu.make_async_copy(pieces.at[p.s], cols.at[p.s], loc.at[2]),
    ]
    for copy in mine:
        copy.start()
    for j in range(2):
        for d in range(1, p.Y):
            t = lax.rem(p.y - d + p.Y, p.Y) * 2 + p.c
            ref = spot(t, j)
            push(ref, ref, ys.at[j, d], yr.at[j, d], p.chip_y(-d)).wait_recv()
            copy = push(ref, ref, ps.at[j, d], pr.at[j, d], p.partner)
            copy.start()
            started.append(copy)
    for j in range(2):
        for d in range(p.Y):
            ref = spot(lax.rem(p.y - d + p.Y, p.Y) * 2 + 1 - p.c, j)
            push(ref, ref, ps.at[j, d], pr.at[j, d], p.partner).wait_recv()
    for e in range(1, sp):
        s = lax.rem(p.s - e + sp, sp)
        push(cols.at[s], cols.at[s], es.at[e], er.at[e], (s, p.t)).wait_recv()
    for copy in started:
        copy.wait_send()
    for copy in mine:
        copy.wait()


def heads_kernel(
    sp, tp, q, hg, small, cols, q_all, hg_all, small_all, cols_all, loc, ys, yr, ps, pr, *line
):
    p = Place(sp, tp)
    greet(
        [p.partner, p.across]
        + [p.chip_y(d) for d in range(1, p.Y)]
        + [p.chip_z(d) for d in range(1, p.Z)]
    )
    gather = LineGather(p, ((q, q_all), (hg, hg_all), (small, small_all)), *line)
    gather.start()
    started = []
    for d in range(1, p.Y):
        copy = push(cols, cols_all.at[:, p.t], ys.at[d], yr.at[d], p.chip_y(d))
        copy.start()
        started.append(copy)
    copy = push(cols, cols_all.at[:, p.t], ps.at[0], pr.at[0], p.partner)
    copy.start()
    started.append(copy)
    mine = [
        pltpu.make_async_copy(q, q_all.at[p.s], loc.at[0]),
        pltpu.make_async_copy(hg, hg_all.at[p.s], loc.at[1]),
        pltpu.make_async_copy(small, small_all.at[p.s], loc.at[2]),
        pltpu.make_async_copy(cols, cols_all.at[:, p.t], loc.at[3]),
    ]
    for copy in mine:
        copy.start()
    for d in range(1, p.Z):
        gather.step(d)
        if d == 1:
            for k in range(1, p.Y):
                ref = cols_all.at[:, lax.rem(p.y - k + p.Y, p.Y) * 2 + p.c]
                push(ref, ref, ys.at[k], yr.at[k], p.chip_y(-k)).wait_recv()
                copy = push(ref, ref, ps.at[k], pr.at[k], p.partner)
                copy.start()
                started.append(copy)
    for k in range(p.Y):
        ref = cols_all.at[:, lax.rem(p.y - k + p.Y, p.Y) * 2 + 1 - p.c]
        push(ref, ref, ps.at[k], pr.at[k], p.partner).wait_recv()
    gather.finish()
    for copy in started:
        copy.wait_send()
    for copy in mine:
        copy.wait()


class PairScatter:
    def __init__(self, p, part, first, summed, second, fs, fr, ss, sr):
        self.p, self.part, self.first, self.summed, self.second = p, part, first, summed, second
        self.sems = (fs, fr, ss, sr)
        self.started = []

    def start(self):
        p = self.p
        for d in range(p.Y):
            y = lax.rem(p.y + d, p.Y)
            copy = push(
                self.part(y * 2 + 1 - p.c), self.first.at[d], self.sems[0].at[d], self.sems[1].at[d], p.partner
            )
            copy.start()
            self.started.append(copy)

    def middle(self):
        p = self.p
        for d in list(range(1, p.Y)) + [0]:
            y = lax.rem(p.y + d, p.Y)
            self.started[d].wait_recv()
            total = self.part(y * 2 + p.c)[...].astype(F32) + self.first[d].astype(F32)
            self.summed[d] = total.astype(BF)
            if d:
                copy = push(
                    self.summed.at[d], self.second.at[d], self.sems[2].at[d], self.sems[3].at[d], p.chip_y(d)
                )
                copy.start()
                self.started.append(copy)

    def finish(self):
        p = self.p
        total = self.part(p.t)[...].astype(F32) + self.first[0].astype(F32)
        for d in range(1, p.Y):
            self.started[p.Y + d - 1].wait_recv()
            total = total + self.second[d].astype(F32)
        for copy in self.started:
            copy.wait_send()
        return total


def grads_kernel(
    sp, tp, part, sg, wq, q_all, src_out, ng_out,
    xr, xz, zr, sg1, sg2, sg3, ng, ng1, ng2, ng3,
    xs_s, xs_r, zs_s, zs_r, a0, a1, a2, a3, b0, b1, b2, b3, *line
):
    p = Place(sp, tp)
    rows = ng1.shape[1]
    greet(
        [p.partner, p.across]
        + [p.chip_y(d) for d in range(1, p.Y)]
        + [p.chip_z(d) for d in range(1, p.Z)]
    )
    started = []
    order = list(range(1, p.Z)) + [0]
    into = {}
    for k in order:
        z = lax.rem(p.z + k, p.Z)
        into[k] = push(part.at[z * 2 + 1 - p.x], xr.at[k], xs_s.at[k], xs_r.at[k], p.across)
        into[k].start()
    source = PairScatter(p, lambda t: sg.at[t], sg1, sg2, sg3, a0, a1, a2, a3)
    source.start()
    source.middle()
    hops = {}
    for k in order[:-1]:
        into[k].wait_recv()
        z = lax.rem(p.z + k, p.Z)
        xz[k] = (part[z * 2 + p.x].astype(F32) + xr[k].astype(F32)).astype(BF)
        hops[k] = push(xz.at[k], zr.at[k], zs_s.at[k], zs_r.at[k], p.chip_z(k))
        hops[k].start()
    into[0].wait_recv()
    total = part[p.s].astype(F32) + xr[0].astype(F32)
    for k in order[:-1]:
        hops[k].wait_recv()
        total = total + zr[k].astype(F32)
    q_all[p.s] = total.astype(BF)
    gather = LineGather(p, ((q_all.at[p.s], q_all),), *line)
    gather.start()
    flat = total.astype(BF)
    width = wq.shape[0]
    tile = min(width, 256)
    for j in range(0, width, tile):
        columns = contract_last(flat, wq[j : j + tile, :]).astype(BF)
        for t in range(tp):
            ng[t, :, j : j + tile] = columns[t * rows : (t + 1) * rows]
    normed = PairScatter(p, lambda t: ng.at[t], ng1, ng2, ng3, b0, b1, b2, b3)
    normed.start()
    for d in range(1, p.Z):
        gather.step(d)
        if d == 1:
            normed.middle()
    src_out[...] = source.finish()
    ng_out[...] = normed.finish()
    gather.finish()
    for k in order:
        into[k].wait_send()
    for k in order[:-1]:
        hops[k].wait_send()


def call(kernel, name, cid, outs, scratch, *args):
    return pl.pallas_call(
        kernel,
        out_shape=[jax.ShapeDtypeStruct(*o) for o in outs],
        in_specs=[VMEM] * len(args),
        out_specs=[VMEM] * len(outs),
        scratch_shapes=scratch,
        name=name,
        compiler_params=pltpu.CompilerParams(
            collective_id=cid, has_side_effects=True, vmem_limit_bytes=56 * 2**20
        ),
    )(*args)


def body(
    target_rows,
    source_rows,
    norm_gain,
    query_weight,
    key_weight,
    value_weight,
    output_weight,
    saved_output,
    norm_offset,
    output_grad,
):
    tp, sp = lax.axis_size("tp"), lax.axis_size("sp")
    Z, Y = sp // 2, tp // 2
    model, width = query_weight.shape
    heads = width // HEAD_DIM
    rows, srows = target_rows.shape[0], source_rows.shape[0]
    block = rows * tp
    count = block * sp
    source_count = srows * tp
    shift_base = math.log(source_count * sp)
    slice_width = model // sp
    dma = pltpu.SemaphoreType.DMA
    scale = HEAD_DIM ** (-0.5)

    target_float = target_rows.astype(F32)
    gain_float = norm_gain.astype(F32)
    inverse = lax.rsqrt(jnp.mean(target_float * target_float, axis=1, keepdims=True) + EPSILON)
    normed = (target_float * inverse * gain_float).astype(BF)
    tgt_all, src_all, cols = call(
        functools.partial(rows_kernel, sp, tp),
        "rows_kernel",
        1,
        [((2, tp, rows, model), BF), ((tp, srows, model), BF), ((sp, rows, slice_width), BF)],
        [dma((3,)), dma((2, Y)), dma((2, Y)), dma((2, Y)), dma((2, Y)), dma((sp,)), dma((sp,))],
        jnp.stack([normed, output_grad]),
        source_rows,
        normed.reshape(rows, sp, slice_width).transpose(1, 0, 2),
    )
    tgt_all = tgt_all.reshape(2, block, model)
    src_all = src_all.reshape(source_count, model)
    query = jnp.dot(tgt_all[0], query_weight, preferred_element_type=F32).astype(BF)
    head_gradient = contract_last(tgt_all[1], output_weight).astype(BF)
    deltas = jnp.sum(
        (head_gradient.astype(F32) * saved_output.astype(F32)).reshape(block, heads, HEAD_DIM), axis=2
    ).astype(BF)
    small = jnp.pad(jnp.concatenate([norm_offset, deltas], axis=1), ((0, 0), (0, 128 - 2 * heads)))
    q_all, hg_all, small_all, cols_all = call(
        functools.partial(heads_kernel, sp, tp),
        "heads_kernel",
        2,
        [
            ((sp, block, width), BF),
            ((sp, block, width), BF),
            ((sp, block, 128), BF),
            ((sp, tp, rows, slice_width), BF),
        ],
        [dma((4,)), dma((Y,)), dma((Y,)), dma((Y,)), dma((Y,))] + line_sems(Z, 3),
        query,
        head_gradient,
        small,
        cols,
    )
    key = jnp.dot(src_all, key_weight, preferred_element_type=F32).astype(BF)
    value = jnp.dot(src_all, value_weight, preferred_element_type=F32).astype(BF)
    q_heads = q_all.reshape(count, heads, HEAD_DIM)
    hg_heads = hg_all.reshape(count, heads, HEAD_DIM)
    k_heads = key.reshape(source_count, heads, HEAD_DIM)
    v_heads = value.reshape(source_count, heads, HEAD_DIM)
    small_rows = small_all.reshape(count, 128).astype(F32)
    offsets = small_rows[:, :heads].T[:, :, None]
    delta_all = small_rows[:, heads : 2 * heads].T[:, :, None]
    scores = jnp.einsum("rfo,kfo->frk", q_heads, k_heads, preferred_element_type=F32)
    prob = jnp.exp(scores * scale - (shift_base + offsets))
    prob_grad = jnp.einsum("rfo,kfo->frk", hg_heads, v_heads, preferred_element_type=F32)
    score_grad = (prob * (prob_grad - delta_all) * scale).astype(BF)
    prob = prob.astype(BF)
    key_flat = (
        jnp.einsum("wcu,cwp->uwp", score_grad, q_heads, preferred_element_type=F32)
        .astype(BF)
        .reshape(source_count, width)
    )
    value_flat = (
        jnp.einsum("wcu,cwp->uwp", prob, hg_heads, preferred_element_type=F32)
        .astype(BF)
        .reshape(source_count, width)
    )
    query_term = jnp.einsum("tje,etq->jtq", score_grad, k_heads, preferred_element_type=F32)
    query_term = query_term.astype(BF).reshape(sp, block, width)
    source_part = (contract_last(key_flat, key_weight) + contract_last(value_flat, value_weight)).astype(BF)
    vm = pltpu.VMEM
    flat_all, source_grad, normed_grad = call(
        functools.partial(grads_kernel, sp, tp),
        "grads_kernel",
        3,
        [((sp, block, width), BF), ((srows, model), F32), ((rows, model), F32)],
        [vm((Z, block, width), BF)] * 3
        + [vm((Y, srows, model), BF)] * 3
        + [vm((tp, rows, model), BF)]
        + [vm((Y, rows, model), BF)] * 3
        + [dma((Z,))] * 4
        + [dma((Y,))] * 8
        + line_sems(Z, 1),
        query_term,
        source_part.reshape(tp, srows, model),
        query_weight,
    )
    scaled = normed_grad * gain_float
    target_grad = inverse * scaled - target_float * inverse**3 * jnp.mean(
        scaled * target_float, axis=1, keepdims=True
    )
    weight_grad = lax.dot_general(
        cols_all.reshape(count, slice_width),
        flat_all.reshape(count, width),
        (((0,), (0,)), ((), ())),
        preferred_element_type=F32,
    )
    return (target_grad, source_grad, weight_grad)


def solution(mesh):
    in_specs = (
        P(("sp", "tp"), None),
        P(("sp", "tp"), None),
        P(),
        P(None, "tp"),
        P(None, "tp"),
        P(None, "tp"),
        P("tp", None),
        P("sp", "tp"),
        P("sp", "tp"),
        P(("sp", "tp"), None),
    )
    out_specs = (P(("sp", "tp"), None), P(("sp", "tp"), None), P("sp", "tp"))
    return jax.shard_map(body, mesh=mesh, in_specs=in_specs, out_specs=out_specs, check_vma=False)
```

time: 431 us -> 136 us (0.32)
  waiting for transfers between devices: 228 us -> 0 us
  blocking collectives: 137 us -> 0 us
  Pallas kernels: 0 us -> 90.9 us
  between operations: 15 us -> 0.9 us
  matrix products: 35.1 us -> 24.4 us
    reduce_scatter x3 -> x0, waiting for transfers between devices: 190 us -> none  [the longest x1 152 us: body(): lax.psum_scatter(lax.dot_general(normed_all, query_flat, (((0,), (0,)), (...]
    unnamed x1 -> x0, blocking collectives: 91.2 us -> none
    pallas_call x0 -> x3, Pallas kernels: none -> 90.9 us  [call(): pl.pallas_call(kernel, out_shape=[jax.ShapeDtypeStruct(*o) for o in outs]...]
    all_gather x3 -> x0, blocking collectives: 45.8 us -> none  [the longest x1 20.8 us: body(): lax.all_gather(norm_offset, 'sp', axis=0, tiled=True)]
    all_gather x3 -> x0, waiting for transfers between devices: 37.2 us -> none  [the longest x1 37.2 us: body(): lax.all_gather(head_gradient, 'sp', axis=0, tiled=True)]
    reshape x4 -> x8, local copies, waits for them, and re-layouts: 1.62 us -> 8.54 us  [the longest x2 3.17 us: body(): hg_heads = hg_all.reshape(count, heads, HEAD_DIM)]
    dot_general x9, matrix products: 23.2 us -> 16.4 us  [the longest x1 4.7 us: body(): jnp.dot(src_all, value_weight, preferred_element_type=F32).astype(BF)]
    dot_general x4 -> x3, matrix products: 12 us -> 8 us  [contract_last(): lax.dot_general(left, right, (((1,), (1,)), ((), ())), preferred_element_...]
  transfers between devices with their start and end apart: 6 -> 0, of which waited for: 4 -> 0; matrix products, arithmetic and copies ran while one was open for 8% -> 0% of each run, Pallas kernels for 0% -> 0%
where the time goes in v1:
time: 136 us
  Pallas kernels  90.9 us (67%)
  matrix products  24.4 us (18%)
  local copies, waits for them, and re-layouts  12.5 us (9%)
  other arithmetic  6.92 us (5%)
    pallas_call x3, Pallas kernels, call(): pl.pallas_call(kernel, out_shape=[jax.ShapeDtypeStruct(*o) for o in outs]...  90.9 us
    dot_general x3, matrix products, contract_last(): lax.dot_general(left, right, (((1,), (1,)), ((), ())), preferred_element_...  8 us
    dot_general x1, matrix products, body(): jnp.dot(src_all, value_weight, preferred_element_type=F32).astype(BF)  4.7 us
    dot_general x1, matrix products, body(): jnp.dot(tgt_all[0], query_weight, preferred_element_type=F32).astype(BF)  3.84 us
    reshape x2, local copies, waits for them, and re-layouts, body(): hg_heads = hg_all.reshape(count, heads, HEAD_DIM)  3.17 us
    unnamed x30, local copies, waits for them, and re-layouts  2.96 us
    reshape x2, local copies, waits for them, and re-layouts, body(): q_heads = q_all.reshape(count, heads, HEAD_DIM)  2.85 us
    dot_general x1, matrix products, body(): lax.dot_general(cols_all.reshape(count, slice_width), flat_all.reshape(co...  2.74 us

profile of v1, /device:TPU:0, one launch (start us, length us, event | category | flops | bytes accessed | tf_op | source)
XLA Modules:
  0.0 135.6 jit_solution(1489251930731317605)
XLA Ops:
  0.6 1.0 fusion.9
  1.6 0.7 convert_element_type.66
  2.3 0.8 copy.51
  3.1 0.9 fusion.45
  4.0 1.5 %pad_maximum_fusion.tgt = bf16[2,16,2048]{2,1,0:T(8,128)(2,1)} fusion(bf16[1,16,2048]{2,1,0:T(8,128)(2,1)} %bitcast.69, bf16[1,16,2048]{2,1,0:T(8,128)(2,1)S(1)} %fusion.45), kind=kLoop, calls=%fused_computation.31 | loop fusion | flops 65536 | bytes 262144 | tf_op jit(solution)/shard_map/stack | solution.py:410
  5.5 0.9 fusion.11
  6.5 0.6 copy.70
  7.1 20.0 %rows_kernel.1 = (bf16[2,4,16,2048]{3,2,1,0:T(8,128)(2,1)}, bf16[4,64,2048]{2,1,0:T(8,128)(2,1)}, bf16[8,16,256]{2,1,0:T(8,128)(2,1)}) custom-call(bf16[2,16,2048]{2,1,0:T(8,128)(2,1)} %pad_maximum_fusion.tgt, bf16[64,2048]{1,0:T(8,128)(2,1)} %src.1, bf16[8,16,256]{2,1,0:T(8,128)(2,1)} %bitcast.67), custom_call_target="tpu_custom_call" | custom-call | tf_op jit(solution)/shard_map/rows_kernel/pallas_call | solution.py:362
  27.1 4.7 %convolution_convert_fusion.3 = bf16[256,1024]{1,0:T(8,128)(2,1)} fusion(bf16[256,2048]{1,0:T(8,128)(2,1)} %bitcast.70, bf16[2048,1024]{1,0:T(8,128)(2,1)} %param.15), kind=kOutput, calls=%fused_computation.9 | convolution fusion | flops 1074003968 | bytes 5767168 | tf_op jit(solution)/shard_map/dot_general | solution.py:439
  31.8 1.3 convolution_convert_fusion.4
  33.4 3.8 %convolution_convert_fusion.6.q = bf16[64,1024]{1,0:T(8,128)(2,1)} fusion(bf16[64,2048]{1,0:T(8,128)(2,1)S(1)} %bitcast.62, bf16[2048,1024]{1,0:T(8,128)(2,1)} %wq.1), kind=kOutput, calls=%fused_computation.12 | convolution fusion | flops 268500992 | bytes 4587520 | tf_op jit(solution)/shard_map/dot_general | solution.py:416
  37.2 2.1 %convert_multiply_fusion = (f32[64,1024]{1,0:T(8,128)S(1)}, bf16[64,1024]{1,0:T(8,128)(2,1)}) fusion(bf16[64,1024]{1,0:T(8,128)(2,1)S(1)} %copy-done.8, bf16[64,2048]{1,0:T(8,128)(2,1)S(1)} %bitcast.61, bf16[1024,2048]{1,0:T(8,128)(2,1)S(1)} %copy-done), kind=kOutput, calls=%fused_computation.20 | convolution fusion | flops 268697600 | bytes 4980736 | tf_op jit(solution)/shard_map/dot_general | solution.py:20
  39.6 0.7 fusion.17.small
  40.3 30.4 %heads_kernel.1 = (bf16[8,64,1024]{2,1,0:T(8,128)(2,1)}, bf16[8,64,1024]{2,1,0:T(8,128)(2,1)}, bf16[8,64,128]{2,1,0:T(8,128)(2,1)}, bf16[8,4,16,256]{3,2,1,0:T(8,128)(2,1)}) custom-call(bf16[64,1024]{1,0:T(8,128)(2,1)} %convolution_convert_fusion.6.q, bf16[64,1024]{1,0:T(8,128)(2,1)} %get-tuple-element.30.hg, bf16[64,128]{1,0:T(8,128)(2,1)} %fusion.17.small, ...), custom_call_target="tpu_custom_call" | custom-call | tf_op jit(solution)/shard_map/heads_kernel/pallas_call | solution.py:362
  70.7 1.9 %reshape.79 = bf16[512,4,256]{2,1,0:T(4,128)(2,1)S(1)} reshape(bf16[8,64,1024]{2,1,0:T(8,128)(2,1)} %get-tuple-element.16) | data formatting | bytes 2097152 | tf_op jit(solution)/shard_map/reshape | solution.py:440
  72.5 1.0 copy.60
  73.9 0.8 copy-done.2
  74.8 1.6 %reshape.80 = bf16[512,4,256]{2,1,0:T(4,128)(2,1)} reshape(bf16[8,64,1024]{2,1,0:T(8,128)(2,1)S(1)} %copy-done.2) | data formatting | bytes 2097152 | tf_op jit(solution)/shard_map/reshape | solution.py:441
  76.3 1.6 %copy.61 = bf16[512,4,256]{0,2,1:T(8,128)(2,1)S(1)} copy(bf16[512,4,256]{2,1,0:T(4,128)(2,1)} %reshape.80) | data formatting | bytes 2097152 | tf_op jit(solution)/shard_map/reshape | solution.py:441
  77.9 0.5 fusion.20
  78.5 0.5 copy-done.13
  79.0 1.0 multiply_convert_fusion
  80.0 0.6 convolution_convert_fusion.1
  80.7 1.2 convolution_convert_fusion.2
  82.4 0.7 copy.59
  83.1 1.5 %reshape.82.part = bf16[8,64,1024]{2,1,0:T(8,128)(2,1)} reshape(bf16[512,4,256]{2,1,0:T(4,128)(2,1)S(1)} %copy.59) | data formatting | bytes 2097152 | tf_op jit(solution)/shard_map/reshape | solution.py:463
  84.7 3.6 %fusion.21 = f32[256,2048]{1,0:T(8,128)S(1)} fusion(bf16[256,1024]{0,1:T(8,128)(2,1)S(1)} %bitcast.65, bf16[2048,1024]{1,0:T(8,128)(2,1)} %param.14), kind=kOutput, calls=%fused_computation.44 | convolution fusion | flops 1073741824 | bytes 6815744 | tf_op jit(solution)/shard_map/dot_general | solution.py:20
  88.3 2.3 %fusion = bf16[256,2048]{1,0:T(8,128)(2,1)} fusion(f32[256,2048]{1,0:T(8,128)S(1)} %fusion.21, bf16[256,1024]{0,1:T(8,128)(2,1)S(1)} %bitcast.64, bf16[2048,1024]{1,0:T(8,128)(2,1)S(1)} %copy-done.11), kind=kOutput, calls=%fused_computation.1 | convolution fusion | flops 1074790400 | bytes 7864320 | tf_op jit(solution)/shard_map/dot_general | solution.py:20
  90.6 40.5 %grads_kernel.1 = (bf16[8,64,1024]{2,1,0:T(8,128)(2,1)}, f32[64,2048]{1,0:T(8,128)}, f32[16,2048]{1,0:T(8,128)}) custom-call(bf16[8,64,1024]{2,1,0:T(8,128)(2,1)} %reshape.82.part, bf16[4,64,2048]{2,1,0:T(8,128)(2,1)} %bitcast.63, bf16[2048,1024]{1,0:T(8,128)(2,1)} %wq.1), custom_call_target="tpu_custom_call" | custom-call | tf_op jit(solution)/shard_map/grads_kernel/pallas_call | solution.py:362
  131.2 2.7 %fusion.22 = f32[256,1024]{1,0:T(8,128)} fusion(bf16[512,256]{1,0:T(8,128)(2,1)S(1)} %bitcast.66, bf16[512,1024]{1,0:T(8,128)(2,1)} %bitcast.60), kind=kOutput, calls=%fused_computation.45 | convolution fusion | flops 268435456 | bytes 2359296 | tf_op jit(solution)/shard_map/dot_general | solution.py:486
  134.0 0.7 fusion.13
  134.8 0.8 copy.72
  (38 shorter events, 1.6 us)
Async XLA Ops:
  27.1 4.7 %copy-start.10 = (bf16[2048,1024]{1,0:T(8,128)(2,1)S(1)}, bf16[2048,1024]{1,0:T(8,128)(2,1)}, u32[]{:S(2)}) copy-start(bf16[2048,1024]{1,0:T(8,128)(2,1)} %param.14) | copy-start | bytes 12582916
  27.1 4.7 %copy-start.12 = (bf16[4,64,2048]{2,1,0:T(8,128)(2,1)S(1)}, bf16[4,64,2048]{2,1,0:T(8,128)(2,1)}, u32[]{:S(2)}) copy-start(bf16[4,64,2048]{2,1,0:T(8,128)(2,1)} %get-tuple-element.13) | copy-start | bytes 3145732
  31.8 1.5 %copy-start.5 = (bf16[2,4,16,2048]{3,2,1,0:T(8,128)(2,1)S(1)}, bf16[2,4,16,2048]{3,2,1,0:T(8,128)(2,1)}, u32[]{:S(2)}) copy-start(bf16[2,4,16,2048]{3,2,1,0:T(8,128)(2,1)} %get-tuple-element.14) | copy-start | bytes 1572868
  33.4 3.9 %copy-start = (bf16[1024,2048]{1,0:T(8,128)(2,1)S(1)}, bf16[1024,2048]{1,0:T(8,128)(2,1)}, u32[]{:S(2)}) copy-start(bf16[1024,2048]{1,0:T(8,128)(2,1)} %param.16) | copy-start | bytes 12582916
  33.4 3.9 %copy-start.8 = (bf16[64,1024]{1,0:T(8,128)(2,1)S(1)}, bf16[64,1024]{1,0:T(8,128)(2,1)}, u32[]{:S(2)}) copy-start(bf16[64,1024]{1,0:T(8,128)(2,1)} %param.17) | copy-start | bytes 393220
  70.6 2.9 %copy-start.9 = (bf16[8,64,128]{2,1,0:T(8,128)(2,1)S(1)}, bf16[8,64,128]{2,1,0:T(8,128)(2,1)}, u32[]{:S(2)}) copy-start(bf16[8,64,128]{2,1,0:T(8,128)(2,1)} %get-tuple-element.17) | copy-start | bytes 393220
  73.5 1.2 copy-start.2
  77.9 1.0 copy-start.13
  82.4 2.3 %copy-start.3 = (bf16[4,256,256]{2,1,0:T(8,128)(2,1)S(1)}, bf16[4,256,256]{2,1,0:T(8,128)(2,1)}, u32[]{:S(2)}) copy-start(bf16[4,256,256]{2,1,0:T(8,128)(2,1)} %convolution_convert_fusion.2) | copy-start | bytes 1572868
  84.7 3.6 %copy-start.11 = (bf16[2048,1024]{1,0:T(8,128)(2,1)S(1)}, bf16[2048,1024]{1,0:T(8,128)(2,1)}, u32[]{:S(2)}) copy-start(bf16[2048,1024]{1,0:T(8,128)(2,1)} %param.15) | copy-start | bytes 12582916
  90.6 40.5 %copy-start.7 = (bf16[8,4,16,256]{3,2,1,0:T(8,128)(2,1)S(1)}, bf16[8,4,16,256]{3,2,1,0:T(8,128)(2,1)}, u32[]{:S(2)}) copy-start(bf16[8,4,16,256]{3,2,1,0:T(8,128)(2,1)} %get-tuple-element.21) | copy-start | bytes 786436
  131.1 2.8 %copy-start.1 = (bf16[16,2048]{1,0:T(8,128)(2,1)S(1)}, bf16[16,2048]{1,0:T(8,128)(2,1)}, u32[]{:S(2)}) copy-start(bf16[16,2048]{1,0:T(8,128)(2,1)} %param.10) | copy-start | bytes 196612
  131.1 2.8 %copy-start.6 = (f32[16,2048]{1,0:T(8,128)S(1)}, f32[16,2048]{1,0:T(8,128)}, u32[]{:S(2)}) copy-start(f32[16,2048]{1,0:T(8,128)} %get-tuple-element.19) | copy-start | bytes 393220
  131.1 3.7 %copy-start.4 = (f32[64,2048]{1,0:T(8,128)S(1)}, f32[64,2048]{1,0:T(8,128)}, u32[]{:S(2)}) copy-start(f32[64,2048]{1,0:T(8,128)} %get-tuple-element.35) | copy-start | bytes 1572868

commit v2 on v1

v2 whole, which is shorter than its diff:
```python
import functools
import math

import jax
import jax.numpy as jnp
from jax import lax
from jax.experimental import pallas as pl
from jax.experimental.pallas import tpu as pltpu
from jax.sharding import PartitionSpec as P

HEAD_DIM = 256
EPSILON = 1e-06
MESH = pl.DeviceIdType.MESH
BF = jnp.bfloat16
F32 = jnp.float32
VMEM = pl.BlockSpec(memory_space=pltpu.VMEM)


def contract_last(left, right):
    return lax.dot_general(left, right, (((1,), (1,)), ((), ())), preferred_element_type=F32)


def push(src, dst, send, recv, device):
    return pltpu.make_async_remote_copy(
        src_ref=src, dst_ref=dst, send_sem=send, recv_sem=recv, device_id=device, device_id_type=MESH
    )


def greet(devices):
    barrier = pltpu.get_barrier_semaphore()
    for device in devices:
        pl.semaphore_signal(barrier, inc=1, device_id=device, device_id_type=MESH)
    pl.semaphore_wait(barrier, len(devices))


class Place:
    def __init__(self, sp, tp):
        self.sp, self.tp, self.Z, self.Y = sp, tp, sp // 2, tp // 2
        self.s, self.t = lax.axis_index("sp"), lax.axis_index("tp")
        self.z, self.x = self.s // 2, self.s % 2
        self.y, self.c = self.t // 2, self.t % 2
        self.partner = (self.s, self.y * 2 + 1 - self.c)
        self.across = (self.z * 2 + 1 - self.x, self.t)

    def chip_y(self, d):
        return (self.s, lax.rem(self.y + d + self.Y, self.Y) * 2 + self.c)

    def chip_z(self, d):
        return (lax.rem(self.z + d + self.Z, self.Z) * 2 + self.x, self.t)


class LineGather:
    def __init__(self, place, pairs, up_s, up_r, dn_s, dn_r, x_s, x_r):
        self.p, self.pairs = place, pairs
        self.sems = (up_s, up_r, dn_s, dn_r, x_s, x_r)

    def up(self, n, d, own=False):
        p, (own_ref, all_ref) = self.p, self.pairs[n]
        block = p.s - 2 * (d - 1)
        src = own_ref if own else all_ref.at[block]
        return push(src, all_ref.at[block], self.sems[0].at[n, d], self.sems[1].at[n, d], (p.s + 2, p.t))

    def up_wait(self, n, d):
        p, (_, all_ref) = self.p, self.pairs[n]
        ref = all_ref.at[p.s - 2 * d]
        return push(ref, ref, self.sems[0].at[n, d], self.sems[1].at[n, d], (p.s - 2, p.t))

    def dn(self, n, d, own=False):
        p, (own_ref, all_ref) = self.p, self.pairs[n]
        block = p.s + 2 * (d - 1)
        src = own_ref if own else all_ref.at[block]
        return push(src, all_ref.at[block], self.sems[2].at[n, d], self.sems[3].at[n, d], (p.s - 2, p.t))

    def dn_wait(self, n, d):
        p, (_, all_ref) = self.p, self.pairs[n]
        ref = all_ref.at[p.s + 2 * d]
        return push(ref, ref, self.sems[2].at[n, d], self.sems[3].at[n, d], (p.s + 2, p.t))

    def over(self, n, d):
        p, (own_ref, all_ref) = self.p, self.pairs[n]
        block = p.s - 2 * d
        k = d + p.Z - 1
        src = own_ref if d == 0 else all_ref.at[block]
        return push(src, all_ref.at[block], self.sems[4].at[n, k], self.sems[5].at[n, k], p.across)

    def over_wait(self, n, d):
        p, (_, all_ref) = self.p, self.pairs[n]
        ref = all_ref.at[p.z * 2 + 1 - p.x - 2 * d]
        k = d + p.Z - 1
        return push(ref, ref, self.sems[4].at[n, k], self.sems[5].at[n, k], p.across)

    def start(self, count):
        p = self.p

        @pl.when(p.z + 1 < p.Z)
        def _():
            for n in count:
                self.up(n, 1, True).start()

        @pl.when(p.z >= 1)
        def _():
            for n in count:
                self.dn(n, 1, True).start()

        for n in count:
            self.over(n, 0).start()

    def step(self, d):
        p = self.p
        for n in range(len(self.pairs)):

            @pl.when(p.z - d >= 0)
            def _():
                self.up_wait(n, d).wait_recv()

                @pl.when(p.z + 1 < p.Z)
                def _():
                    self.up(n, d + 1).start()

                self.over(n, d).start()

            @pl.when(p.z + d < p.Z)
            def _():
                self.dn_wait(n, d).wait_recv()

                @pl.when(p.z >= 1)
                def _():
                    self.dn(n, d + 1).start()

                self.over(n, -d).start()

    def arrive(self, sign, d):
        for n in range(len(self.pairs)):
            self.over_wait(n, sign * d).wait_recv()

    def side(self, sign, d):
        return self.p.z - d >= 0 if sign > 0 else self.p.z + d < self.p.Z

    def finish(self):
        p = self.p
        for n in range(len(self.pairs)):
            for d in range(p.Z):
                for sign in (1, -1) if d else (1,):

                    @pl.when(self.side(sign, d))
                    def _():
                        self.over(n, sign * d).wait_send()

            for d in range(1, p.Z):

                @pl.when(jnp.logical_and(p.z - d + 1 >= 0, p.z + 1 < p.Z))
                def _():
                    self.up(n, d).wait_send()

                @pl.when(jnp.logical_and(p.z + d - 1 < p.Z, p.z >= 1))
                def _():
                    self.dn(n, d).wait_send()


def line_sems(p_z, n):
    return [pltpu.SemaphoreType.DMA((n, p_z + 1))] * 4 + [pltpu.SemaphoreType.DMA((n, 2 * p_z))] * 2


class PairScatter:
    def __init__(self, p, part, first, summed, second, fs, fr, ss, sr):
        self.p, self.part, self.first, self.summed, self.second = p, part, first, summed, second
        self.sems = (fs, fr, ss, sr)
        self.started = []

    def start(self):
        p = self.p
        for d in range(p.Y):
            y = lax.rem(p.y + d, p.Y)
            copy = push(
                self.part(y * 2 + 1 - p.c), self.first.at[d], self.sems[0].at[d], self.sems[1].at[d], p.partner
            )
            copy.start()
            self.started.append(copy)

    def middle(self):
        p = self.p
        for d in list(range(1, p.Y)) + [0]:
            y = lax.rem(p.y + d, p.Y)
            self.started[d].wait_recv()
            total = self.part(y * 2 + p.c)[...].astype(F32) + self.first[d].astype(F32)
            self.summed[d] = total.astype(BF)
            if d:
                copy = push(
                    self.summed.at[d], self.second.at[d], self.sems[2].at[d], self.sems[3].at[d], p.chip_y(d)
                )
                copy.start()
                self.started.append(copy)

    def finish(self):
        p = self.p
        total = self.part(p.t)[...].astype(F32) + self.first[0].astype(F32)
        for d in range(1, p.Y):
            self.started[p.Y + d - 1].wait_recv()
            total = total + self.second[d].astype(F32)
        for copy in self.started:
            copy.wait_send()
        return total


class PairGather:
    def __init__(self, p, own, spot, ys, yr, ps, pr):
        self.p, self.own, self.spot, self.sems = p, own, spot, (ys, yr, ps, pr)
        self.started = []

    def start(self):
        p = self.p
        for d in range(1, p.Y):
            copy = push(self.own, self.spot(p.t), self.sems[0].at[d], self.sems[1].at[d], p.chip_y(d))
            copy.start()
            self.started.append(copy)
        copy = push(self.own, self.spot(p.t), self.sems[2].at[0], self.sems[3].at[0], p.partner)
        copy.start()
        self.started.append(copy)

    def forward(self):
        p = self.p
        for d in range(1, p.Y):
            ref = self.spot(lax.rem(p.y - d + p.Y, p.Y) * 2 + p.c)
            push(ref, ref, self.sems[0].at[d], self.sems[1].at[d], p.chip_y(-d)).wait_recv()
            copy = push(ref, ref, self.sems[2].at[d], self.sems[3].at[d], p.partner)
            copy.start()
            self.started.append(copy)

    def arrive(self):
        p = self.p
        for d in range(p.Y):
            ref = self.spot(lax.rem(p.y - d + p.Y, p.Y) * 2 + 1 - p.c)
            push(ref, ref, self.sems[2].at[d], self.sems[3].at[d], p.partner).wait_recv()

    def finish(self):
        for copy in self.started:
            copy.wait_send()


def layer_kernel(
    sp, tp, shift_base,
    tn, to, src, pieces, saved, offs, wq_h, wk_h, wv_h, wo_h,
    flat_all, src_out, ng_out, cols_all,
    wq, wk, wv, wo, tn_all, to_all, src_all, cols, tn_b, to_b,
    q_all, hg_all, small_all, k_s, v_s, p_s, d_s, part, kf, vf, sg,
    xr, xz, zr, sg1, sg2, sg3, ng, ng1, ng2, ng3,
    wsem, loc, es, er, *sems
):
    p = Place(sp, tp)
    pair_sems = [sems[4 * i : 4 * i + 4] for i in range(6)]
    xs_s, xs_r, zs_s, zs_r = sems[24:28]
    line_a, line_b = sems[28:34], sems[34:40]
    rows, block = tn.shape[0], saved.shape[0]
    width, model = wq.shape[1], wq.shape[0]
    heads = width // HEAD_DIM
    scale = HEAD_DIM ** (-0.5)
    loads = [
        pltpu.make_async_copy(h, v, wsem.at[i])
        for i, (h, v) in enumerate(((wq_h, wq), (wo_h, wo), (wk_h, wk), (wv_h, wv)))
    ]
    for copy in loads:
        copy.start()
    greet(
        [p.partner]
        + [p.chip_y(d) for d in range(1, p.Y)]
        + [(lax.rem(p.s + e, sp), p.t) for e in range(1, sp)]
    )
    g_tn = PairGather(p, tn, lambda t: tn_all.at[t], *pair_sems[0])
    g_to = PairGather(p, to, lambda t: to_all.at[t], *pair_sems[1])
    g_src = PairGather(p, src, lambda t: src_all.at[t], *pair_sems[2])
    g_cols = PairGather(p, cols, lambda t: cols_all.at[:, t], *pair_sems[3])
    for g in (g_tn, g_to, g_src):
        g.start()
    swaps = []
    for e in range(1, sp):
        s = lax.rem(p.s + e, sp)
        copy = push(pieces.at[s], cols.at[p.s], es.at[e], er.at[e], (s, p.t))
        copy.start()
        swaps.append(copy)
    mine = [
        pltpu.make_async_copy(tn, tn_all.at[p.t], loc.at[0]),
        pltpu.make_async_copy(to, to_all.at[p.t], loc.at[1]),
        pltpu.make_async_copy(src, src_all.at[p.t], loc.at[2]),
        pltpu.make_async_copy(pieces.at[p.s], cols.at[p.s], loc.at[3]),
    ]
    for copy in mine:
        copy.start()
    for copy in mine:
        copy.wait()
    tile = min(width, 256)
    gather = LineGather(
        p, ((q_all.at[p.s], q_all), (hg_all.at[p.s], hg_all), (small_all.at[p.s], small_all)), *line_a
    )

    g_tn.forward()
    g_to.forward()
    g_tn.arrive()
    for t in range(tp):
        tn_b[t * rows : (t + 1) * rows, :] = tn_all[t]
    loads[0].wait()
    for j in range(0, width, tile):
        q_all[p.s, :, j : j + tile] = jnp.dot(
            tn_b[...], wq[:, j : j + tile], preferred_element_type=F32
        ).astype(BF)
    gather.start((0,))
    g_to.arrive()
    for t in range(tp):
        to_b[t * rows : (t + 1) * rows, :] = to_all[t]
    loads[1].wait()
    lane = lax.broadcasted_iota(jnp.int32, (block, 128), 1)
    small = jnp.zeros((block, 128), F32)
    off_value = offs[...].astype(F32)
    for h in range(heads):
        cut = slice(h * HEAD_DIM, (h + 1) * HEAD_DIM)
        part_h = contract_last(to_b[...], wo[cut, :]).astype(BF)
        hg_all[p.s, :, cut] = part_h
        delta = jnp.sum(part_h.astype(F32) * saved[:, cut].astype(F32), axis=1, keepdims=True)
        small = jnp.where(lane == h, off_value[:, h : h + 1], small)
        small = jnp.where(lane == heads + h, delta, small)
    small_all[p.s] = small.astype(BF)
    gather.start((1, 2))

    g_src.forward()
    g_src.arrive()
    source_count = k_s.shape[0]
    loads[2].wait()
    loads[3].wait()

    @pl.loop(0, width // tile)
    def _(j):
        cut = pl.ds(pl.multiple_of(j * tile, tile), tile)
        rows_value = src_all[...].reshape(source_count, model)
        k_s[:, cut] = jnp.dot(rows_value, wk[:, cut], preferred_element_type=F32).astype(BF)
        v_s[:, cut] = jnp.dot(rows_value, wv[:, cut], preferred_element_type=F32).astype(BF)

    for e in range(1, sp):
        s = lax.rem(p.s - e + sp, sp)
        push(cols.at[s], cols.at[s], es.at[e], er.at[e], (s, p.t)).wait_recv()
    g_cols.start()
    keep = pltpu.make_async_copy(cols, cols_all.at[:, p.t], loc.at[4])
    keep.start()

    def into(k):
        z = lax.rem(p.z + k, p.Z)
        return push(part.at[z * 2 + 1 - p.x], xr.at[k], xs_s.at[k], xs_r.at[k], p.across)

    def attend(z):
        pair = pl.ds(2 * z, 2)
        spot = pl.ds(pl.multiple_of(z * (2 * block), 2 * block), 2 * block)
        tiny = small_all[pair].reshape(2 * block, 128).astype(F32)
        for h in range(heads):
            cut = slice(h * HEAD_DIM, (h + 1) * HEAD_DIM)
            q_h = q_all[pair, :, cut].reshape(2 * block, HEAD_DIM)
            g_h = hg_all[pair, :, cut].reshape(2 * block, HEAD_DIM)
            prob = jnp.exp(contract_last(q_h, k_s[:, cut]) * scale - (shift_base + tiny[:, h : h + 1]))
            grad = contract_last(g_h, v_s[:, cut])
            score = (prob * (grad - tiny[:, heads + h : heads + h + 1]) * scale).astype(BF)
            p_s[h, spot, :] = prob.astype(BF)
            d_s[h, spot, :] = score
            term = jnp.dot(score, k_s[:, cut], preferred_element_type=F32).astype(BF)
            part[pair, :, cut] = term.reshape(2, block, HEAD_DIM)

    def reached(sign, d):
        gather.arrive(sign, d)
        attend(p.z - sign * d)
        into((-sign * d) % p.Z).start()

    for d in range(1, p.Z):
        gather.step(d)
        for sign in (1, -1) if d > 1 else (1,):

            @pl.when(gather.side(sign, d - 1))
            def _():
                reached(sign, d - 1)

        if d == 1:
            g_cols.forward()
    for sign in (1, -1):

        @pl.when(gather.side(sign, p.Z - 1))
        def _():
            reached(sign, p.Z - 1)

    order = sorted(range(1, p.Z), key=lambda k: min(k, p.Z - k))
    hops = {}

    def relay(k):
        into(k).wait_recv()
        z = lax.rem(p.z + k, p.Z)
        xz[k] = (part[z * 2 + p.x].astype(F32) + xr[k].astype(F32)).astype(BF)
        hops[k] = push(xz.at[k], zr.at[k], zs_s.at[k], zs_r.at[k], p.chip_z(k))
        hops[k].start()

    for k in order[:1]:
        relay(k)
    count = sp * block

    for h in range(heads):
        cut = slice(h * HEAD_DIM, (h + 1) * HEAD_DIM)
        dims = (((0,), (0,)), ((), ()))
        q_h = q_all[:, :, cut].reshape(count, HEAD_DIM)
        g_h = hg_all[:, :, cut].reshape(count, HEAD_DIM)
        kf[:, cut] = lax.dot_general(d_s[h], q_h, dims, preferred_element_type=F32).astype(BF)
        vf[:, cut] = lax.dot_general(p_s[h], g_h, dims, preferred_element_type=F32).astype(BF)
    for k in order[1:2]:
        relay(k)
    stile = min(model, 256)

    @pl.loop(0, model // stile)
    def _(j):
        cut = pl.ds(pl.multiple_of(j * stile, stile), stile)
        value = contract_last(kf[...], wk[cut, :]) + contract_last(vf[...], wv[cut, :])
        sg[:, :, cut] = value.astype(BF).reshape(tp, source_count // tp, stile)

    source = PairScatter(p, lambda t: sg.at[t], sg1, sg2, sg3, *pair_sems[4])
    source.start()
    for k in order[2:]:
        relay(k)
    source.middle()
    into(0).wait_recv()
    total = part[p.s].astype(F32) + xr[0].astype(F32)
    for k in order:
        hops[k].wait_recv()
        total = total + zr[k].astype(F32)
    flat = total.astype(BF)
    flat_all[p.s] = flat
    spread = LineGather(p, ((flat_all.at[p.s], flat_all),), *line_b)
    spread.start((0,))
    for j in range(0, model, stile):
        columns = contract_last(flat, wq[j : j + stile, :]).astype(BF)
        for t in range(tp):
            ng[t, :, j : j + stile] = columns[t * rows : (t + 1) * rows]
    normed = PairScatter(p, lambda t: ng.at[t], ng1, ng2, ng3, *pair_sems[5])
    normed.start()
    for d in range(1, p.Z):
        spread.step(d)
        if d == 1:
            normed.middle()
    src_out[...] = source.finish()
    ng_out[...] = normed.finish()
    g_cols.arrive()
    for d in range(p.Z):
        for sign in (1, -1) if d else (1,):

            @pl.when(spread.side(sign, d))
            def _():
                spread.arrive(sign, d)

    gather.finish()
    spread.finish()
    for g in (g_tn, g_to, g_src, g_cols):
        g.finish()
    for copy in swaps:
        copy.wait_send()
    keep.wait()
    for k in range(p.Z):
        into(k).wait_send()
    for k in order:
        hops[k].wait_send()


def body(
    target_rows,
    source_rows,
    norm_gain,
    query_weight,
    key_weight,
    value_weight,
    output_weight,
    saved_output,
    norm_offset,
    output_grad,
):
    tp, sp = lax.axis_size("tp"), lax.axis_size("sp")
    Z, Y = sp // 2, tp // 2
    model, width = query_weight.shape
    heads = width // HEAD_DIM
    rows, srows = target_rows.shape[0], source_rows.shape[0]
    block = rows * tp
    count = block * sp
    source_count = srows * tp
    shift_base = math.log(source_count * sp)
    slice_width = model // sp
    dma = pltpu.SemaphoreType.DMA

    target_float = target_rows.astype(F32)
    gain_float = norm_gain.astype(F32)
    inverse = lax.rsqrt(jnp.mean(target_float * target_float, axis=1, keepdims=True) + EPSILON)
    normed = (target_float * inverse * gain_float).astype(BF)
    vm = pltpu.VMEM
    whole = pl.BlockSpec(memory_space=pl.ANY)
    flat_all, source_grad, normed_grad, cols_all = pl.pallas_call(
        functools.partial(layer_kernel, sp, tp, shift_base),
        out_shape=[
            jax.ShapeDtypeStruct((sp, block, width), BF),
            jax.ShapeDtypeStruct((srows, model), F32),
            jax.ShapeDtypeStruct((rows, model), F32),
            jax.ShapeDtypeStruct((sp, tp, rows, slice_width), BF),
        ],
        in_specs=[VMEM] * 6 + [whole] * 4,
        out_specs=[VMEM] * 4,
        scratch_shapes=[vm((model, width), BF)] * 3
        + [vm((width, model), BF)]
        + [vm((tp, rows, model), BF)] * 2
        + [vm((tp, srows, model), BF), vm((sp, rows, slice_width), BF)]
        + [vm((block, model), BF)] * 2
        + [vm((sp, block, width), BF)] * 2
        + [vm((sp, block, 128), BF)]
        + [vm((source_count, width), BF)] * 2
        + [vm((heads, count, source_count), BF)] * 2
        + [vm((sp, block, width), BF)]
        + [vm((source_count, width), BF)] * 2
        + [vm((tp, srows, model), BF)]
        + [vm((Z, block, width), BF)] * 3
        + [vm((Y, srows, model), BF)] * 3
        + [vm((tp, rows, model), BF)]
        + [vm((Y, rows, model), BF)] * 3
        + [dma((4,)), dma((5,)), dma((sp,)), dma((sp,))]
        + [dma((Y,))] * 24
        + [dma((Z,))] * 4
        + line_sems(Z, 3)
        + line_sems(Z, 1),
        name="layer_kernel",
        compiler_params=pltpu.CompilerParams(
            collective_id=1, has_side_effects=True, vmem_limit_bytes=58 * 2**20
        ),
    )(
        normed,
        output_grad,
        source_rows,
        normed.reshape(rows, sp, slice_width).transpose(1, 0, 2),
        saved_output,
        norm_offset,
        query_weight,
        key_weight,
        value_weight,
        output_weight,
    )
    scaled = normed_grad * gain_float
    target_grad = inverse * scaled - target_float * inverse**3 * jnp.mean(
        scaled * target_float, axis=1, keepdims=True
    )
    weight_grad = lax.dot_general(
        cols_all.reshape(count, slice_width),
        flat_all.reshape(count, width),
        (((0,), (0,)), ((), ())),
        preferred_element_type=F32,
    )
    return (target_grad, source_grad, weight_grad)


def solution(mesh):
    in_specs = (
        P(("sp", "tp"), None),
        P(("sp", "tp"), None),
        P(),
        P(None, "tp"),
        P(None, "tp"),
        P(None, "tp"),
        P("tp", None),
        P("sp", "tp"),
        P("sp", "tp"),
        P(("sp", "tp"), None),
    )
    out_specs = (P(("sp", "tp"), None), P(("sp", "tp"), None), P("sp", "tp"))
    return jax.shard_map(body, mesh=mesh, in_specs=in_specs, out_specs=out_specs, check_vma=False)
```

time: 136 us -> 96.8 us (0.71)
  matrix products: 24.4 us -> 2.75 us
  local copies, waits for them, and re-layouts: 12.5 us -> 3.9 us
  Pallas kernels: 90.9 us -> 83.9 us
  other arithmetic: 6.92 us -> 5.29 us
    dot_general x11 -> x0, matrix products: 21.7 us -> none  [the longest x3 8 us: contract_last(): lax.dot_general(left, right, (((1,), (1,)), ((), ())), preferred_element_...]
    reshape x7 -> x0, local copies, waits for them, and re-layouts: 7.9 us -> none  [the longest x2 3.17 us: body(): hg_heads = hg_all.reshape(count, heads, HEAD_DIM)]
    pallas_call x3 -> x1, Pallas kernels: 90.9 us -> 83.9 us  [body(): pl.pallas_call(functools.partial(layer_kernel, sp, tp, shift_base), out_s...]
    another operation x2 -> x0, other arithmetic: 2.43 us -> none  [body(): jnp.stack([normed, output_grad])]
    unnamed x30 -> x6, local copies, waits for them, and re-layouts: 2.96 us -> 3.26 us
where the time goes in v2:
time: 96.8 us; the launch traced here: 96.5 us
  Pallas kernels  83.9 us (87%)
  other arithmetic  5.29 us (5%)
  local copies, waits for them, and re-layouts  3.9 us (4%)
  matrix products  2.75 us (3%)
    pallas_call x1, Pallas kernels, body(): pl.pallas_call(functools.partial(layer_kernel, sp, tp, shift_base), out_s...  83.9 us
    unnamed x6, local copies, waits for them, and re-layouts  3.26 us
    dot_general x1, matrix products, body(): lax.dot_general(cols_all.reshape(count, slice_width), flat_all.reshape(co...  2.75 us

profile of v2, /device:TPU:0, one launch (start us, length us, event | category | flops | bytes accessed | tf_op | source)
XLA Modules:
  0.0 96.5 jit_solution(9665309107495569253)
XLA Ops:
  0.6 0.7 convert_element_type.10
  1.3 1.0 %fusion = f32[16]{0:T(128)S(1)} fusion(bf16[16,2048]{1,0:T(8,128)(2,1)} %param.10), kind=kLoop, calls=%fused_computation.4 | loop fusion | flops 98288 | bytes 65600 | tf_op jit(solution)/shard_map/reduce_sum | solution.py:488
  2.3 0.9 fusion.2.tn
  3.2 0.0 copy-start.1
  3.2 0.6 copy.18
  3.9 1.4 %copy.15.offs = bf16[64,4]{1,0:T(8,128)(2,1)} copy(bf16[64,4]{0,1:T(4,128)(2,1)} %param.18) | data formatting | bytes 1024 | tf_op args[8]
  5.3 0.0 copy-done.1
  5.3 0.0 copy-start
  5.3 83.9 %layer_kernel.1 = (bf16[8,64,1024]{2,1,0:T(8,128)(2,1)}, f32[64,2048]{1,0:T(8,128)}, f32[16,2048]{1,0:T(8,128)}, bf16[8,4,16,256]{3,2,1,0:T(8,128)(2,1)}) custom-call(bf16[16,2048]{1,0:T(8,128)(2,1)} %copy-done.1, bf16[16,2048]{1,0:T(8,128)(2,1)} %to.1, bf16[64,2048]{1,0:T(8,128)(2,1)} %src.1, bf16[8,16,256]{2,1,0:T(8,128)(2,1)} %bitcast.13, ...), custom_call_target="tpu_custom_call" | custom-call | tf_op jit(solution)/shard_map/layer_kernel/pallas_call | solution.py:492
  89.1 0.0 copy-done
  89.1 1.0 %fusion.5 = f32[16]{0:T(128)S(1)} fusion(bf16[16,2048]{1,0:T(8,128)(2,1)S(1)} %copy-done, f32[16,2048]{1,0:T(8,128)} %get-tuple-element.7, f32[2048]{0:T(1024)S(1)} %convert_element_type.10), kind=kLoop, calls=%fused_computation.9 | loop fusion | flops 131056 | bytes 204864 | tf_op jit(solution)/shard_map/reduce_sum | solution.py:540
  90.2 1.7 %fusion.4 = f32[16,2048]{1,0:T(8,128)} fusion(bf16[16,2048]{1,0:T(8,128)(2,1)S(1)} %copy-done, f32[16,2048]{1,0:T(8,128)} %get-tuple-element.7, f32[16]{0:T(128)S(1)} %broadcast_multiply_fusion, f32[16]{0:T(128)S(1)} %get-tuple-element.11, f32[2048]{0:T(1024)S(1)} %convert_element_type.10, f32[16]{0:T(128)S(1)} %get-tuple-element.12), kind=kLoop, calls=%fused_computation.8 | loop fusion | flops 196608 | bytes 336064 | tf_op jit(solution)/shard_map/sub | solution.py:540
  91.8 2.8 %fusion.6 = f32[256,1024]{1,0:T(8,128)} fusion(bf16[512,256]{1,0:T(8,128)(2,1)} %bitcast.14, bf16[512,1024]{1,0:T(8,128)(2,1)} %bitcast.11), kind=kOutput, calls=%fused_computation.14 | convolution fusion | flops 268435456 | bytes 2359296 | tf_op jit(solution)/shard_map/dot_general | solution.py:543
  94.6 1.9 %copy.20 = f32[64,2048]{1,0:T(8,128)} copy(f32[64,2048]{1,0:T(8,128)} %get-tuple-element.17) | data formatting | bytes 1048576
  (2 shorter events, 0.0 us)
Async XLA Ops:
  3.2 2.0 %copy-start.1 = (bf16[16,2048]{1,0:T(8,128)(2,1)}, bf16[16,2048]{1,0:T(8,128)(2,1)S(1)}, u32[]{:S(2)}) copy-start(bf16[16,2048]{1,0:T(8,128)(2,1)S(1)} %fusion.2.tn) | copy-start | bytes 196612
  5.3 83.9 %copy-start = (bf16[16,2048]{1,0:T(8,128)(2,1)S(1)}, bf16[16,2048]{1,0:T(8,128)(2,1)}, u32[]{:S(2)}) copy-start(bf16[16,2048]{1,0:T(8,128)(2,1)} %param.10) | copy-start | bytes 196612

commit v3 on v2

--- a/solution.py
+++ b/solution.py
@@ -239,9 +239,9 @@
 
 def layer_kernel(
     sp, tp, shift_base,
-    tn, to, src, pieces, saved, offs, wq_h, wk_h, wv_h, wo_h,
-    flat_all, src_out, ng_out, cols_all,
-    wq, wk, wv, wo, tn_all, to_all, src_all, cols, tn_b, to_b,
+    raw, to, src, gain, saved, offs, wq_h, wk_h, wv_h, wo_h,
+    flat_all, src_out, tgt_out, cols_all,
+    tn, pieces, wq, wk, wv, wo, tn_all, to_all, src_all, cols, tn_b, to_b,
     q_all, hg_all, small_all, k_s, v_s, p_s, d_s, part, kf, vf, sg,
     xr, xz, zr, sg1, sg2, sg3, ng, ng1, ng2, ng3,
     wsem, loc, es, er, *sems
@@ -250,7 +250,7 @@
     pair_sems = [sems[4 * i : 4 * i + 4] for i in range(6)]
     xs_s, xs_r, zs_s, zs_r = sems[24:28]
     line_a, line_b = sems[28:34], sems[34:40]
-    rows, block = tn.shape[0], saved.shape[0]
+    rows, block = raw.shape[0], saved.shape[0]
     width, model = wq.shape[1], wq.shape[0]
     heads = width // HEAD_DIM
     scale = HEAD_DIM ** (-0.5)
@@ -260,6 +260,13 @@
     ]
     for copy in loads:
         copy.start()
+    raw_value, gain_value = raw[...].astype(F32), gain[...].astype(F32)
+    inverse = lax.rsqrt(jnp.mean(raw_value * raw_value, axis=1, keepdims=True) + EPSILON)
+    normed_value = (raw_value * inverse * gain_value).astype(BF)
+    tn[...] = normed_value
+    slice_width = model // sp
+    for s in range(sp):
+        pieces[s] = normed_value[:, s * slice_width : (s + 1) * slice_width]
     greet(
         [p.partner]
         + [p.chip_y(d) for d in range(1, p.Y)]
@@ -308,20 +315,23 @@
         to_b[t * rows : (t + 1) * rows, :] = to_all[t]
     loads[1].wait()
     lane = lax.broadcasted_iota(jnp.int32, (block, 128), 1)
-    small = jnp.zeros((block, 128), F32)
-    off_value = offs[...].astype(F32)
+    pick = lax.broadcasted_iota(jnp.int32, (heads, 128), 0) == lax.broadcasted_iota(jnp.int32, (heads, 128), 1)
+    small = lax.dot_general(
+        offs[...].astype(F32), pick.astype(F32), (((0,), (0,)), ((), ())), precision=lax.Precision.HIGHEST,
+        preferred_element_type=F32,
+    )
     for h in range(heads):
         cut = slice(h * HEAD_DIM, (h + 1) * HEAD_DIM)
         part_h = contract_last(to_b[...], wo[cut, :]).astype(BF)
         hg_all[p.s, :, cut] = part_h
         delta = jnp.sum(part_h.astype(F32) * saved[:, cut].astype(F32), axis=1, keepdims=True)
-        small = jnp.where(lane == h, off_value[:, h : h + 1], small)
         small = jnp.where(lane == heads + h, delta, small)
     small_all[p.s] = small.astype(BF)
     gather.start((1, 2))
 
     g_src.forward()
     g_src.arrive()
+    gather.step(1)
     source_count = k_s.shape[0]
     loads[2].wait()
     loads[3].wait()
@@ -366,7 +376,8 @@
         into((-sign * d) % p.Z).start()
 
     for d in range(1, p.Z):
-        gather.step(d)
+        if d > 1:
+            gather.step(d)
         for sign in (1, -1) if d > 1 else (1,):
 
             @pl.when(gather.side(sign, d - 1))
@@ -406,16 +417,18 @@
         relay(k)
     stile = min(model, 256)
 
-    @pl.loop(0, model // stile)
-    def _(j):
+    def source_term(j):
         cut = pl.ds(pl.multiple_of(j * stile, stile), stile)
         value = contract_last(kf[...], wk[cut, :]) + contract_last(vf[...], wv[cut, :])
         sg[:, :, cut] = value.astype(BF).reshape(tp, source_count // tp, stile)
 
+    half = model // stile // 2
+    pl.loop(0, half)(source_term)
+    for k in order[2:]:
+        relay(k)
+    pl.loop(half, model // stile)(source_term)
     source = PairScatter(p, lambda t: sg.at[t], sg1, sg2, sg3, *pair_sems[4])
     source.start()
-    for k in order[2:]:
-        relay(k)
     source.middle()
     into(0).wait_recv()
     total = part[p.s].astype(F32) + xr[0].astype(F32)
@@ -437,7 +450,12 @@
         if d == 1:
             normed.middle()
     src_out[...] = source.finish()
-    ng_out[...] = normed.finish()
+    raw_value, gain_value = raw[...].astype(F32), gain[...].astype(F32)
+    inverse = lax.rsqrt(jnp.mean(raw_value * raw_value, axis=1, keepdims=True) + EPSILON)
+    scaled = normed.finish() * gain_value
+    tgt_out[...] = inverse * scaled - raw_value * (inverse * inverse * inverse) * jnp.mean(
+        scaled * raw_value, axis=1, keepdims=True
+    )
     g_cols.arrive()
     for d in range(p.Z):
         for sign in (1, -1) if d else (1,):
@@ -483,13 +501,9 @@
     slice_width = model // sp
     dma = pltpu.SemaphoreType.DMA
 
-    target_float = target_rows.astype(F32)
-    gain_float = norm_gain.astype(F32)
-    inverse = lax.rsqrt(jnp.mean(target_float * target_float, axis=1, keepdims=True) + EPSILON)
-    normed = (target_float * inverse * gain_float).astype(BF)
     vm = pltpu.VMEM
     whole = pl.BlockSpec(memory_space=pl.ANY)
-    flat_all, source_grad, normed_grad, cols_all = pl.pallas_call(
+    flat_all, source_grad, target_grad, cols_all = pl.pallas_call(
         functools.partial(layer_kernel, sp, tp, shift_base),
         out_shape=[
             jax.ShapeDtypeStruct((sp, block, width), BF),
@@ -499,7 +513,8 @@
         ],
         in_specs=[VMEM] * 6 + [whole] * 4,
         out_specs=[VMEM] * 4,
-        scratch_shapes=[vm((model, width), BF)] * 3
+        scratch_shapes=[vm((rows, model), BF), vm((sp, rows, slice_width), BF)]
+        + [vm((model, width), BF)] * 3
         + [vm((width, model), BF)]
         + [vm((tp, rows, model), BF)] * 2
         + [vm((tp, srows, model), BF), vm((sp, rows, slice_width), BF)]
@@ -525,20 +540,16 @@
             collective_id=1, has_side_effects=True, vmem_limit_bytes=58 * 2**20
         ),
     )(
-        normed,
+        target_rows,
         output_grad,
         source_rows,
-        normed.reshape(rows, sp, slice_width).transpose(1, 0, 2),
+        norm_gain.reshape(1, model),
         saved_output,
-        norm_offset,
+        norm_offset.T,
         query_weight,
         key_weight,
         value_weight,
         output_weight,
-    )
-    scaled = normed_grad * gain_float
-    target_grad = inverse * scaled - target_float * inverse**3 * jnp.mean(
-        scaled * target_float, axis=1, keepdims=True
     )
     weight_grad = lax.dot_general(
         cols_all.reshape(count, slice_width),

time: 96.8 us -> 89.4 us (0.924)
  other arithmetic: 5.29 us -> 0 us
  Pallas kernels: 83.9 us -> 81 us
    pallas_call x1, Pallas kernels: 83.9 us -> 81 us  [body(): pl.pallas_call(functools.partial(layer_kernel, sp, tp, shift_base), out_s...]
    reduce_sum x2 -> x0, other arithmetic: 2 us -> none  [the longest x1 1.04 us: body(): jnp.mean(scaled * target_float, axis=1, keepdims=True)]
    sub x1 -> x0, other arithmetic: 1.65 us -> none  [body(): inverse * scaled]
    convert_element_type x2 -> x0, other arithmetic: 1.62 us -> none  [the longest x1 0.93 us: body(): normed = (target_float * inverse * gain_float).astype(BF)]
    unnamed x6 -> x2, local copies, waits for them, and re-layouts: 3.26 us -> 3.44 us
where the time goes in v3:
time: 89.4 us; the launch traced here: 89.2 us
  Pallas kernels  81 us (91%)
  local copies, waits for them, and re-layouts  4.73 us (5%)
  matrix products  2.76 us (3%)
    pallas_call x1, Pallas kernels, body(): pl.pallas_call(functools.partial(layer_kernel, sp, tp, shift_base), out_s...  81 us
    unnamed x2, local copies, waits for them, and re-layouts  3.44 us
    dot_general x1, matrix products, body(): lax.dot_general(cols_all.reshape(count, slice_width), flat_all.reshape(co...  2.76 us

profile of v3, /device:TPU:0, one launch (start us, length us, event | category | flops | bytes accessed | tf_op | source)
XLA Modules:
  0.0 89.2 jit_solution(9263265205593608787)
XLA Ops:
  0.6 1.3 %reshape.15.gain = bf16[1,2048]{1,0:T(2,128)(2,1)} reshape(bf16[2048]{0:T(1024)(128)(2,1)} %param.12) | data formatting | bytes 8192 | tf_op jit(solution)/shard_map/reshape | solution.py:546
  1.9 81.0 %layer_kernel.1 = (bf16[8,64,1024]{2,1,0:T(8,128)(2,1)}, f32[64,2048]{1,0:T(8,128)}, f32[16,2048]{1,0:T(8,128)}, bf16[8,4,16,256]{3,2,1,0:T(8,128)(2,1)}) custom-call(bf16[16,2048]{1,0:T(8,128)(2,1)} %raw.1, bf16[16,2048]{1,0:T(8,128)(2,1)} %to.1, bf16[64,2048]{1,0:T(8,128)(2,1)} %src.1, bf16[1,2048]{1,0:T(2,128)(2,1)} %reshape.15.gain, ...), custom_call_target="tpu_custom_call" | custom-call | tf_op jit(solution)/shard_map/layer_kernel/pallas_call | solution.py:506
  83.0 2.8 %fusion = f32[256,1024]{1,0:T(8,128)} fusion(bf16[512,256]{1,0:T(8,128)(2,1)} %bitcast.6, bf16[512,1024]{1,0:T(8,128)(2,1)} %bitcast.5), kind=kOutput, calls=%fused_computation | convolution fusion | flops 268435456 | bytes 2359296 | tf_op jit(solution)/shard_map/dot_general | solution.py:554
  85.7 1.6 %copy.15 = f32[16,2048]{1,0:T(8,128)} copy(f32[16,2048]{1,0:T(8,128)} %get-tuple-element.14) | data formatting | bytes 262144
  87.3 1.9 %copy.16 = f32[64,2048]{1,0:T(8,128)} copy(f32[64,2048]{1,0:T(8,128)} %get-tuple-element.15) | data formatting | bytes 1048576
